TPU v7x, 32 devices: a whole 2x2x4 slice. The times are simulated.
32 devices in a mesh: ep: 32 (over z, y, x, core).
Axes of the slice: x: 2, y: 2, z: 4, core: 2. Of those that a mesh axis runs over, the one named last changes fastest.
Arguments:
- tokens: bfloat16 [4096, 2048], P('ep'), may hold values from -6 to 6
- norm_gain: float32 [2048], replicated, may hold values from 0.1 to 1.9
- route_ids: int32 [4096, 2], P('ep'), may hold values from 0 to 31, all different within a row; in each aligned block of 128 rows (0 to 127, 128 to 255, ...) at most 8 rows name the same one
- route_weight: float32 [4096, 2], P('ep'), may hold values from 0.25 to 1
- expert_gate: bfloat16 [32, 2048, 1024], P('ep'), may hold values from -0.125 to 0.125
- expert_up: bfloat16 [32, 2048, 1024], P('ep'), may hold values from -0.125 to 0.125
- expert_down: bfloat16 [32, 1024, 2048], P('ep'), may hold values from -0.1875 to 0.1875
- dense_up: bfloat16 [2048, 512], P('ep'), may hold values from -0.125 to 0.125
- dense_down: bfloat16 [512, 2048], P(None, 'ep'), may hold values from -0.25 to 0.25
- branch_gate: float32 [2048], replicated, may hold values from -1.5 to 1.5
Outputs:
- mixed: bfloat16 [4096, 2048], P('ep')
Inputs may be any that keep to these rules, and one draw needn't show every extreme that they name: `route_ids`: each token names 2 different experts; among the 128 tokens of one device (aligned blocks of rows) no expert is named more than 8 times, and in every draw some expert is named exactly 8 times by some device's tokens; every expert is named by some token.
All inputs are finite; a program needn't handle non-finite values.
Results may differ from a plain program's by a relative error of at most 0.01.
Values may be sent and summed in bfloat16 or wider, within the bound.
A program may use at most 128 MiB of HBM per device.

v0:
```python
import jax
import jax.numpy as jnp
from jax import lax
from jax.sharding import PartitionSpec as P

CAP = 8


def taken_in(piece, axis, dim, hop, start):
    def gathered(part):
        return lax.all_gather(part, axis, axis=dim, tiled=True)

    return hop(start, jax.tree.map(gathered, piece), jnp.int32(0))


def on_whole(value, axis, dim, block):
    whole = lax.all_gather(value, axis, axis=dim, tiled=True)
    return block(whole, jnp.int32(0))


def dense_branch(normed, dense_up, dense_down):

    def add_rows(carry_sum, row_piece, row_start):
        columns = lax.dynamic_slice_in_dim(normed, row_start, row_piece.shape[0], 1)
        return carry_sum + jnp.dot(columns, row_piece, preferred_element_type=jnp.float32)

    empty = jnp.zeros((normed.shape[0], dense_up.shape[1]), jnp.float32)
    dense_pre = taken_in(dense_up, "ep", 0, add_rows, empty)
    dense_hidden = jax.nn.silu(dense_pre).astype(jnp.bfloat16)

    def project(col_piece, col_start):
        return jnp.dot(dense_hidden, col_piece, preferred_element_type=jnp.float32)

    return on_whole(dense_down, "ep", 1, project)


def on_device(
    tokens,
    norm_gain,
    route_ids,
    route_weight,
    expert_gate,
    expert_up,
    expert_down,
    dense_up,
    dense_down,
    branch_gate,
):
    n_dev = lax.axis_size("ep")
    tok_rows = tokens.shape[0]
    top_count = route_ids.shape[1]
    exp_local = expert_gate.shape[0]
    experts = exp_local * n_dev
    width = tokens.shape[1]
    wide_tokens = tokens.astype(jnp.float32)
    scale = lax.rsqrt(jnp.mean(wide_tokens * wide_tokens, axis=-1, keepdims=True) + 1e-06)
    normed = (wide_tokens * scale * norm_gain).astype(jnp.bfloat16)
    flat_ids = route_ids.reshape(-1).astype(jnp.int32)
    onehot = (flat_ids[:, None] == jnp.arange(experts, dtype=jnp.int32)[None, :]).astype(jnp.int32)
    earlier = jnp.cumsum(onehot, axis=0) - onehot
    slot_index = jnp.sum(earlier * onehot, axis=-1).astype(jnp.int32)
    position = (flat_ids * CAP + slot_index).astype(jnp.int32)
    token_index = (jnp.arange(tok_rows * top_count, dtype=jnp.int32) // top_count).astype(jnp.int32)
    place_table = (
        jnp.zeros((experts * CAP, tok_rows), jnp.bfloat16).at[position, token_index].set(1.0)
    )
    buffer = jnp.dot(place_table, normed, preferred_element_type=jnp.float32).astype(jnp.bfloat16)
    buffer = buffer.reshape(n_dev, exp_local * CAP, width)
    received = lax.all_to_all(buffer, "ep", split_axis=0, concat_axis=0, tiled=True)
    dense_out = dense_branch(normed, dense_up, dense_down)
    expert_rows = (
        received.reshape(n_dev, exp_local, CAP, width)
        .transpose(1, 0, 2, 3)
        .reshape(exp_local, n_dev * CAP, width)
    )
    gate_part = jnp.einsum(
        "erd,edf->erf", expert_rows, expert_gate, preferred_element_type=jnp.float32
    )
    up_part = jnp.einsum("erd,edf->erf", expert_rows, expert_up, preferred_element_type=jnp.float32)
    hidden = (jax.nn.silu(gate_part) * up_part).astype(jnp.bfloat16)
    results = jnp.einsum(
        "erf,efd->erd", hidden, expert_down, preferred_element_type=jnp.float32
    ).astype(jnp.bfloat16)
    outgoing = (
        results.reshape(exp_local, n_dev, CAP, width)
        .transpose(1, 0, 2, 3)
        .reshape(n_dev, exp_local * CAP, width)
    )
    returned = lax.all_to_all(outgoing, "ep", split_axis=0, concat_axis=0, tiled=True)
    returned = returned.reshape(experts * CAP, width)
    picked = jnp.take(returned, position, axis=0).astype(jnp.float32)
    picked = picked.reshape(tok_rows, top_count, width)
    combined = jnp.sum(picked * route_weight[:, :, None], axis=1)
    return (combined + jnp.tanh(branch_gate) * dense_out).astype(jnp.bfloat16)


def solution(mesh):
    placed = (
        P("ep", None),
        P(),
        P("ep", None),
        P("ep", None),
        P("ep", None, None),
        P("ep", None, None),
        P("ep", None, None),
        P("ep", None),
        P(None, "ep"),
        P(),
    )
    return jax.shard_map(
        on_device, mesh=mesh, in_specs=placed, out_specs=P("ep", None), check_vma=False
    )
```

profile of v0, /device:TPU:0, one launch (start us, length us, event | category | flops | bytes accessed | tf_op | source)
XLA Modules:
  0.0 143.7 jit_solution(7377943106249082075)
XLA Ops:
  6.5 0.7 all-gather.3.cloned.1.call-update
  7.3 0.8 copy.18
  8.2 0.1 reshape.151
  8.3 0.6 reduce-window.6
  8.9 0.2 slice_reduce_fusion
  9.2 0.7 broadcast_multiply_fusion
  10.0 0.1 mul.73
  10.3 12.4 %scatter_fusion = bf16[256,128]{1,0:T(8,128)(2,1)S(1)} fusion(bf16[256,128]{1,0:T(8,128)(2,1)S(1)} %broadcast_in_dim.24, s32[256]{0:T(256)S(1)} %bitcast.57, bf16[256]{0:T(256)(128)(2,1)S(1)} %broadcast.154), kind=kCustom, calls=%fused_computation.1 | custom fusion | bytes 3584 | tf_op jit(solution)/shard_map/scatter | solution.py:65
  22.7 0.2 fusion.21
  22.9 1.5 %fusion.12 = bf16[32,8,2048]{2,1,0:T(8,128)(2,1)} fusion(bf16[256,128]{1,0:T(8,128)(2,1)S(1)} %scatter_fusion, bf16[128,2048]{1,0:T(8,128)(2,1)S(1)} %copy-done, f32[2048]{0:T(1024)S(1)} %copy-done.2, f32[128]{0:T(128)S(1)} %add_rsqrt_fusion), kind=kOutput, calls=%fused_computation.11 | convolution fusion | flops 135790592 | bytes 1647104 | tf_op jit(solution)/shard_map/dot_general | solution.py:67
  24.4 7.4 %all-to-all-start = ((bf16[32,8,2048]{2,1,0:T(8,128)(2,1)}), bf16[32,8,2048]{2,1,0:T(8,128)(2,1)S(1)}, u32[]{:S(2)}, u32[]{:S(2)}) async-start(bf16[32,8,2048]{2,1,0:T(8,128)(2,1)} %fusion.12), calls=%async_computation | async-start | bytes 2097152 | tf_op jit(solution)/shard_map/all_to_all | solution.py:69
  31.8 0.7 all-gather.5.cloned.1.call-update
  32.5 29.3 %all-to-all-done = bf16[32,8,2048]{2,1,0:T(8,128)(2,1)S(1)} async-done(((bf16[32,8,2048]{2,1,0:T(8,128)(2,1)}), bf16[32,8,2048]{2,1,0:T(8,128)(2,1)S(1)}, u32[]{:S(2)}, u32[]{:S(2)}) %all-to-all-start) | async-done | bytes 1048608 | tf_op jit(solution)/shard_map/all_to_all | solution.py:69
  61.8 4.4 %fusion.4 = f32[256,1024]{1,0:T(8,128)} fusion(bf16[1,2048,1024]{2,1,0:T(8,128)(2,1)} %param.14, bf16[32,8,2048]{2,1,0:T(8,128)(2,1)S(1)} %all-to-all-done), kind=kOutput, calls=%fused_computation.6 | convolution fusion | flops 1073741824 | bytes 6291456 | tf_op jit(solution)/shard_map/erd,edf->erf/dot_general | solution.py:76
  66.2 7.2 %fusion.9 = bf16[32,8,2048]{2,1,0:T(8,128)(2,1)} fusion(bf16[1,1024,2048]{2,1,0:T(8,128)(2,1)} %param.16, bf16[1,2048,1024]{2,1,0:T(8,128)(2,1)} %param.15, bf16[32,8,2048]{2,1,0:T(8,128)(2,1)S(1)} %all-to-all-done, f32[256,1024]{1,0:T(8,128)} %fusion.4), kind=kOutput, calls=%fused_computation.10 | convolution fusion | flops 2149580800 | bytes 11534336 | tf_op jit(solution)/shard_map/erf,efd->erd/dot_general | solution.py:81
  73.5 5.4 %all-to-all-start.1 = ((bf16[32,8,2048]{2,1,0:T(8,128)(2,1)}), bf16[32,8,2048]{2,1,0:T(8,128)(2,1)S(1)}, u32[]{:S(2)}, u32[]{:S(2)}) async-start(bf16[32,8,2048]{2,1,0:T(8,128)(2,1)} %fusion.9), calls=%async_computation.1 | async-start | bytes 2097152 | tf_op jit(solution)/shard_map/all_to_all | solution.py:89
  78.8 0.1 reduce_sum.32
  79.1 0.1 copy.22
  79.4 28.4 %all-to-all-done.1 = bf16[32,8,2048]{2,1,0:T(8,128)(2,1)S(1)} async-done(((bf16[32,8,2048]{2,1,0:T(8,128)(2,1)}), bf16[32,8,2048]{2,1,0:T(8,128)(2,1)S(1)}, u32[]{:S(2)}, u32[]{:S(2)}) %all-to-all-start.1) | async-done | bytes 1048608 | tf_op jit(solution)/shard_map/all_to_all | solution.py:89
  107.8 1.4 gather_fusion
  109.1 0.7 gather.7
  109.9 4.1 %multiply_reduce_fusion = f32[128,2048]{1,0:T(8,128)S(1)} fusion(bf16[128,2,2048]{2,1,0:T(2,128)(2,1)S(1)} %gather.7, pred[128,2]{1,0:T(8,128)(4,1)S(1)} %copy.22, f32[128,2]{1,0:T(8,128)S(1)} %copy.24), kind=kLoop, calls=%fused_computation.15 | loop fusion | flops 1835008 | bytes 2098432 | tf_op jit(solution)/shard_map/reduce_sum | solution.py:93
  114.0 18.7 %all-gather.5.cloned.1.call-done = bf16[512,2048]{0,1:T(8,128)(2,1)} async-done(((bf16[512,64]{0,1:T(8,128)(2,1)}), bf16[512,2048]{0,1:T(8,128)(2,1)}) %all-gather.5.cloned.1.call-update) | async-done | bytes 2097168 | tf_op jit(solution)/shard_map/all_gather | solution.py:17
  132.6 4.2 %fusion.14 = bf16[128,2048]{1,0:T(8,128)(2,1)} fusion(f32[128,2048]{1,0:T(8,128)S(1)} %multiply_reduce_fusion, bf16[512,2048]{0,1:T(8,128)(2,1)} %all-gather.5.cloned.1.call-done, f32[2048]{0:T(1024)S(1)} %tanh.3, bf16[2048,512]{1,0:T(8,128)(2,1)} %all-gather.3.cloned.1.call-done, bf16[128,2048]{1,0:T(8,128)(2,1)S(1)} %copy-done, f32[2048]{0:T(1024)S(1)} %copy-done.2, ...), kind=kOutput, calls=%fused_computation.14 | convolution fusion | flops 539033600 | bytes 6308352 | tf_op jit(solution)/shard_map/dot_general | solution.py:32
  (28 shorter events, 0.7 us)
Async XLA Ops:
  6.5 16.1 %copy-start = (bf16[128,2048]{1,0:T(8,128)(2,1)S(1)}, bf16[128,2048]{1,0:T(8,128)(2,1)}, u32[]{:S(2)}) copy-start(bf16[128,2048]{1,0:T(8,128)(2,1)} %param.10) | copy-start | bytes 1572868
  6.5 16.3 %copy-start.2 = (f32[2048]{0:T(1024)S(1)}, f32[2048]{0:T(1024)}, u32[]{:S(2)}) copy-start(f32[2048]{0:T(1024)} %param.11) | copy-start | bytes 24580
  6.5 107.4 %all-gather.3.cloned.1.call-start = ((), (), s32[]{:S(2)}) async-start(), calls=%async_computation.2 | async-start | bytes 2162688 | tf_op jit(solution)/shard_map/all_gather | solution.py:11
  24.4 37.5 %all-to-all-start = ((bf16[32,8,2048]{2,1,0:T(8,128)(2,1)}), bf16[32,8,2048]{2,1,0:T(8,128)(2,1)S(1)}, u32[]{:S(2)}, u32[]{:S(2)}) async-start(bf16[32,8,2048]{2,1,0:T(8,128)(2,1)} %fusion.12), calls=%async_computation | async-start | bytes 2097152 | tf_op jit(solution)/shard_map/all_to_all | solution.py:69
  31.8 100.9 %all-gather.5.cloned.1.call-start = ((), (), s32[]{:S(2)}) async-start(), calls=%async_computation.3 | async-start | bytes 2162688 | tf_op jit(solution)/shard_map/all_gather | solution.py:17
  73.5 5.6 %copy-start.1 = (s32[128,2]{0,1:T(2,128)S(1)}, s32[128,2]{0,1:T(2,128)}, u32[]{:S(2)}) copy-start(s32[128,2]{0,1:T(2,128)} %param.12) | copy-start | bytes 3076
  73.5 5.7 %copy-start.4 = (f32[128,2]{0,1:T(2,128)S(1)}, f32[128,2]{0,1:T(2,128)}, u32[]{:S(2)}) copy-start(f32[128,2]{0,1:T(2,128)} %param.13) | copy-start | bytes 3076
  73.5 5.9 %copy-start.3 = (f32[2048]{0:T(1024)S(1)}, f32[2048]{0:T(1024)}, u32[]{:S(2)}) copy-start(f32[2048]{0:T(1024)} %param.19) | copy-start | bytes 24580
  73.5 34.3 %all-to-all-start.1 = ((bf16[32,8,2048]{2,1,0:T(8,128)(2,1)}), bf16[32,8,2048]{2,1,0:T(8,128)(2,1)S(1)}, u32[]{:S(2)}, u32[]{:S(2)}) async-start(bf16[32,8,2048]{2,1,0:T(8,128)(2,1)} %fusion.9), calls=%async_computation.1 | async-start | bytes 2097152 | tf_op jit(solution)/shard_map/all_to_all | solution.py:89
Sparse Core Ops, SparseCore 0:
  10.2 61.9 all-gather.2
  75.0 57.5 all-gather.4
where the time goes:
time: 144 us
  waiting for transfers between devices  77.8 us (54%)
  matrix products  17.4 us (12%)
  local copies, waits for them, and re-layouts  16.5 us (11%)
  between operations  13.5 us (9%)
  starting transfers between devices  12.8 us (9%)
  other arithmetic  5.72 us (4%)
    all_to_all x1, waiting for transfers between devices, on_device(): lax.all_to_all(buffer, 'ep', split_axis=0, concat_axis=0, tiled=True)  29.3 us
    all_to_all x1, waiting for transfers between devices, on_device(): lax.all_to_all(outgoing, 'ep', split_axis=0, concat_axis=0, tiled=True)  28.4 us
    all_gather x1, waiting for transfers between devices, on_whole(): whole = lax.all_gather(value, axis, axis=dim, tiled=True)  18.7 us
    scatter x1, local copies, waits for them, and re-layouts, on_device(): jnp.zeros((experts * CAP, tok_rows), jnp.bfloat16).at[position, token_index]  12.4 us
    all_to_all x1, starting transfers between devices, on_device(): lax.all_to_all(buffer, 'ep', split_axis=0, concat_axis=0, tiled=True)  7.39 us
    dot_general x1, matrix products, on_device(): jnp.einsum('erf,efd->erd', hidden, expert_down, preferred_element_type=jn...  7.24 us
    all_to_all x1, starting transfers between devices, on_device(): lax.all_to_all(outgoing, 'ep', split_axis=0, concat_axis=0, tiled=True)  5.35 us
    dot_general x1, matrix products, on_device(): jnp.einsum('erd,edf->erf', expert_rows, expert_gate, preferred_element_ty...  4.41 us
  transfers between devices with their start and end apart: 4, of which 3 were waited for; matrix products, arithmetic and copies ran while one was open for 25% of the time, Pallas kernels for 0%

commit v1 on v0

v1 whole, which is shorter than its diff:
```python
import functools
import math

import jax
import jax.numpy as jnp
from jax import lax
from jax.experimental import pallas as pl
from jax.experimental.pallas import tpu as pltpu
from jax.sharding import PartitionSpec as P

CAP = 8
F32 = jnp.float32
BF16 = jnp.bfloat16


def xor(a, b, size):
    out, bit = 0, 1
    while bit < size:
        out = out + ((a // bit) % 2 + (b // bit) % 2) % 2 * bit
        bit *= 2
    return out


def kernel(
    dims,
    tokens, gain, ids, weight, w_gate, w_up, w_down, d_up, d_down, branch,
    out,
    normed, send, recv, result, back, v_gate, v_up, v_down, wide,
    local_sem, out_send, out_recv, ret_send, ret_recv,
    z_send, z_recv, y_send, y_recv, x_send, x_recv, c_send, c_recv,
):
    n_z, n_y, n_x, n_c = dims
    plane = n_y * n_x * n_c
    n = n_z * plane
    me = lax.axis_index("ep")
    my_z = me // plane
    my_in = me % plane
    my_c = me % n_c
    my_x = me // n_c % n_x
    my_y = me // (n_c * n_x) % n_y
    rows = tokens.shape[0]
    width = tokens.shape[1]
    experts = n
    slots = experts * CAP

    def dev(z, y, x, c):
        return ((z * n_y + y) * n_x + x) * n_c + c

    barrier = pltpu.get_barrier_semaphore()

    def greet(i, carry):
        pl.semaphore_signal(barrier, inc=1, device_id=((me + i) % n,), device_id_type=pl.DeviceIdType.MESH)
        return carry

    lax.fori_loop(1, n, greet, 0)

    own_up = pltpu.make_async_copy(d_up, wide.at[0, my_z, my_y, my_x, my_c], local_sem.at[0])
    own_down = pltpu.make_async_copy(d_down, wide.at[1, my_z, my_y, my_x, my_c], local_sem.at[1])
    own_up.start()
    own_down.start()
    loads = [
        pltpu.make_async_copy(w_gate.at[0], v_gate, local_sem.at[2]),
        pltpu.make_async_copy(w_up.at[0], v_up, local_sem.at[3]),
        pltpu.make_async_copy(w_down.at[0], v_down, local_sem.at[4]),
    ]
    for load in loads:
        load.start()

    x = tokens[...].astype(F32)
    scale = lax.rsqrt(jnp.mean(x * x, axis=-1, keepdims=True) + 1e-06)
    normed[...] = (x * scale * gain[...]).astype(BF16)

    id0, id1 = ids[0:1, :], ids[1:2, :]
    e_iota = lax.broadcasted_iota(jnp.int32, (experts, rows), 0)
    hot0 = (id0 == e_iota).astype(F32)
    hot1 = (id1 == e_iota).astype(F32)
    before = lax.broadcasted_iota(jnp.int32, (rows, rows), 0) < lax.broadcasted_iota(jnp.int32, (rows, rows), 1)
    count = jnp.dot((hot0 + hot1).astype(BF16), before.astype(F32).astype(BF16), preferred_element_type=F32)
    pos0 = id0 * CAP + jnp.sum(hot0 * count, axis=0, keepdims=True).astype(jnp.int32)
    pos1 = id1 * CAP + jnp.sum(hot1 * count, axis=0, keepdims=True).astype(jnp.int32)
    p_iota = lax.broadcasted_iota(jnp.int32, (slots, rows), 0)
    table0 = (pos0 == p_iota).astype(F32)
    table1 = (pos1 == p_iota).astype(F32)
    place = (table0 + table1).astype(BF16)
    packed = jnp.dot(place, normed[...], preferred_element_type=F32)
    send[...] = packed.reshape(n, CAP, width).astype(BF16)

    own_up.wait()
    own_down.wait()
    pl.semaphore_wait(barrier, n - 1)

    def remote(src, dst, s, r, target):
        return pltpu.make_async_remote_copy(
            src_ref=src, dst_ref=dst, send_sem=s, recv_sem=r,
            device_id=(target,), device_id_type=pl.DeviceIdType.MESH,
        )

    def z_copy(d, origin):
        part = wide.at[:, origin, my_y, my_x, my_c]
        return remote(part, part, z_send.at[d], z_recv.at[d], dev((my_z + d) % n_z, my_y, my_x, my_c))

    def y_copy(d, origin):
        part = wide.at[:, :, origin, my_x, my_c]
        return remote(part, part, y_send.at[d], y_recv.at[d], dev(my_z, (my_y + d) % n_y, my_x, my_c))

    def x_copy(d, origin):
        part = wide.at[:, :, :, origin, my_c]
        return remote(part, part, x_send.at[d], x_recv.at[d], dev(my_z, my_y, (my_x + d) % n_x, my_c))

    def c_copy(d, origin):
        part = wide.at[:, :, :, :, origin]
        return remote(part, part, c_send.at[d], c_recv.at[d], dev(my_z, my_y, my_x, (my_c + d) % n_c))

    stages = [(z_copy, n_z, my_z), (y_copy, n_y, my_y), (x_copy, n_x, my_x), (c_copy, n_c, my_c)]

    def begin(stage):
        copy, size, at = stages[stage]
        for d in range(1, size):
            copy(d, at).start()

    def arrive(stage):
        copy, size, at = stages[stage]
        for d in range(1, size):
            copy(d, (at + size - d) % size).wait_recv()

    def leave(stage):
        copy, size, at = stages[stage]
        for d in range(1, size):
            copy(d, at).wait_send()

    begin(0)

    def partner(step):
        z = xor(my_z, (step // plane + n_z // 2) % n_z, n_z)
        return z * plane + xor(my_in, step % plane, plane)

    own_step = (n_z - n_z // 2) * plane

    def over_others(first, last, body):
        def guarded(step, carry):
            body(partner(step))
            return carry

        if first <= own_step < last:
            lax.fori_loop(first, own_step, guarded, 0)
            lax.fori_loop(own_step + 1, last, guarded, 0)
        else:
            lax.fori_loop(first, last, guarded, 0)

    def dispatch(target, origin):
        return remote(send.at[target], recv.at[origin], out_send.at[target], out_recv.at[origin], target)

    def giveback(target, origin):
        return remote(result.at[target], back.at[origin], ret_send.at[target], ret_recv.at[origin], target)

    over_others(0, n, lambda t: dispatch(t, me).start())
    recv[me] = send[me]

    for load in loads:
        load.wait()

    def experts_on(phase):
        z = xor(my_z, (phase + n_z // 2) % n_z, n_z)
        block = pl.ds(z * plane, plane)
        x_in = recv[block].reshape(plane * CAP, width)
        gate_part = jnp.dot(x_in, v_gate[...], preferred_element_type=F32)
        up_part = jnp.dot(x_in, v_up[...], preferred_element_type=F32)
        hidden = (gate_part / (1.0 + jnp.exp(-gate_part)) * up_part).astype(BF16)
        res = jnp.dot(hidden, v_down[...], preferred_element_type=F32)
        result[block] = res.reshape(plane, CAP, width).astype(BF16)

    arrive(0)
    begin(1)

    def do_phase(phase):
        lo, hi = phase * plane, (phase + 1) * plane
        over_others(lo, hi, lambda t: dispatch(me, t).wait_recv())
        experts_on(phase)
        over_others(lo, hi, lambda t: giveback(t, me).start())

    for phase in range(n_z):
        do_phase(phase)
        if phase < 3:
            arrive(phase + 1)
            if phase < 2:
                begin(phase + 2)

    back[me] = result[me]

    dense_pre = jnp.dot(normed[...], wide[0].reshape(width, -1), preferred_element_type=F32)
    dense_hidden = (dense_pre / (1.0 + jnp.exp(-dense_pre))).astype(BF16)
    dense_out = lax.dot_general(
        dense_hidden, wide[1].reshape(width, -1), (((1,), (1,)), ((), ())), preferred_element_type=F32
    )
    dense_out = jnp.tanh(branch[...]) * dense_out

    share = table0 * weight[0:1, :] + table1 * weight[1:2, :]
    high = share.astype(BF16)
    low = (share - high.astype(F32)).astype(BF16)

    over_others(0, n, lambda t: giveback(me, t).wait_recv())
    rows_back = back[...].reshape(slots, width)
    across = (((0,), (0,)), ((), ()))
    combined = lax.dot_general(high, rows_back, across, preferred_element_type=F32)
    combined = combined + lax.dot_general(low, rows_back, across, preferred_element_type=F32)
    out[...] = (combined + dense_out).astype(BF16)

    over_others(0, n, lambda t: dispatch(t, me).wait_send())
    over_others(0, n, lambda t: giveback(t, me).wait_send())
    for stage in range(4):
        leave(stage)


def on_device(tokens, norm_gain, route_ids, route_weight, expert_gate, expert_up, expert_down, dense_up, dense_down, branch_gate):
    n = lax.axis_size("ep")
    assert expert_gate.shape[0] == 1
    rows, width = tokens.shape
    ff = expert_gate.shape[2]
    d_rows, dh = dense_up.shape
    n_z = 4
    side = math.isqrt(n // n_z // 2)
    dims = (n_z, side, side, 2)
    assert math.prod(dims) == n
    vmem = pl.BlockSpec(memory_space=pltpu.VMEM)
    hbm = pl.BlockSpec(memory_space=pl.ANY)
    dma = pltpu.SemaphoreType.DMA
    return pl.pallas_call(
        functools.partial(kernel, dims),
        out_shape=jax.ShapeDtypeStruct((rows, width), BF16),
        in_specs=[vmem, vmem, vmem, vmem, hbm, hbm, hbm, hbm, hbm, vmem],
        out_specs=vmem,
        scratch_shapes=[
            pltpu.VMEM((rows, width), BF16),
            pltpu.VMEM((n, CAP, width), BF16),
            pltpu.VMEM((n, CAP, width), BF16),
            pltpu.VMEM((n, CAP, width), BF16),
            pltpu.VMEM((n, CAP, width), BF16),
            pltpu.VMEM((width, ff), BF16),
            pltpu.VMEM((width, ff), BF16),
            pltpu.VMEM((ff, width), BF16),
            pltpu.VMEM((2,) + dims + (d_rows, dh), BF16),
            dma((5,)), dma((n,)), dma((n,)), dma((n,)), dma((n,)),
            dma((n_z,)), dma((n_z,)), dma((side,)), dma((side,)),
            dma((side,)), dma((side,)), dma((2,)), dma((2,)),
        ],
        compiler_params=pltpu.CompilerParams(
            collective_id=0, has_side_effects=True, vmem_limit_bytes=60 * 1024 * 1024
        ),
    )(
        tokens, norm_gain.reshape(1, -1), route_ids.T, route_weight.T,
        expert_gate, expert_up, expert_down, dense_up, dense_down.T, branch_gate.reshape(1, -1),
    )


def solution(mesh):
    placed = (
        P("ep", None), P(), P("ep", None), P("ep", None),
        P("ep", None, None), P("ep", None, None), P("ep", None, None),
        P("ep", None), P(None, "ep"), P(),
    )
    return jax.shard_map(
        on_device, mesh=mesh, in_specs=placed, out_specs=P("ep", None), check_vma=False
    )
```

time: 144 us -> 102 us (0.71)
  Pallas kernels: 0 us -> 99.8 us
  waiting for transfers between devices: 77.8 us -> 0 us
  matrix products: 17.4 us -> 0 us
  local copies, waits for them, and re-layouts: 16.5 us -> 1.88 us
  between operations: 13.5 us -> 0.01 us
  starting transfers between devices: 12.8 us -> 0 us
  other arithmetic: 5.72 us -> 0 us
    pallas_call x0 -> x1, Pallas kernels: none -> 99.8 us  [on_device(): pl.pallas_call(functools.partial(kernel, dims), out_shape=jax.ShapeDtypeS...]
    all_to_all x2 -> x0, waiting for transfers between devices: 57.7 us -> none  [the longest x1 29.3 us: on_device(): lax.all_to_all(buffer, 'ep', split_axis=0, concat_axis=0, tiled=True)]
    all_gather x2 -> x0, waiting for transfers between devices: 18.7 us -> none  [the longest x1 18.7 us: on_whole(): whole = lax.all_gather(value, axis, axis=dim, tiled=True)]
    dot_general x4 -> x0, matrix products: 17.4 us -> none  [the longest x1 7.24 us: on_device(): jnp.einsum('erf,efd->erd', hidden, expert_down, preferred_element_type=jn...]
    all_to_all x2 -> x0, starting transfers between devices: 12.7 us -> none  [the longest x1 7.39 us: on_device(): lax.all_to_all(buffer, 'ep', split_axis=0, concat_axis=0, tiled=True)]
    scatter x1 -> x0, local copies, waits for them, and re-layouts: 12.4 us -> none  [on_device(): jnp.zeros((experts * CAP, tok_rows), jnp.bfloat16).at[position, token_index]]
    reduce_sum x3 -> x0, other arithmetic: 4.36 us -> none  [the longest x1 4.07 us: on_device(): combined = jnp.sum(picked * route_weight[:, :, None], axis=1)]
    gather x2 -> x0, local copies, waits for them, and re-layouts: 2.07 us -> none  [on_device(): picked = jnp.take(returned, position, axis=0).astype(jnp.float32)]
  transfers between devices with their start and end apart: 4 -> 0, of which waited for: 3 -> 0; matrix products, arithmetic and copies ran while one was open for 25% -> 0% of each run, Pallas kernels for 0% -> 0%
where the time goes in v1:
time: 102 us
  Pallas kernels  99.8 us (98%)
  local copies, waits for them, and re-layouts  1.88 us (2%)
    pallas_call x1, Pallas kernels, on_device(): pl.pallas_call(functools.partial(kernel, dims), out_shape=jax.ShapeDtypeS...  99.8 us

profile of v1, /device:TPU:0, one launch (start us, length us, event | category | flops | bytes accessed | tf_op | source)
XLA Modules:
  0.0 101.7 jit_solution(5517678846801833181)
XLA Ops:
  0.0 99.8 %shard_map.100 = bf16[128,2048]{1,0:T(8,128)(2,1)} custom-call(bf16[128,2048]{1,0:T(8,128)(2,1)} %tokens.1, f32[1,2048]{1,0:T(1,128)} %bitcast.6, s32[2,128]{1,0:T(2,128)} %bitcast.8, f32[2,128]{1,0:T(2,128)} %bitcast.9, bf16[1,2048,1024]{2,1,0:T(8,128)(2,1)} %w_gate.1, bf16[1,2048,1024]{2,1,0:T(8,128)(2,1)} %w_up.1, bf16[1,1024,2048]{2,1,0:T(8,128)(2,1)} %w_down.1, ...), custom_call_target="tpu_custom_call" | custom-call | tf_op jit(solution)/shard_map/pallas_call | solution.py:227
  99.8 1.9 %copy.12 = bf16[128,2048]{1,0:T(8,128)(2,1)} copy(bf16[128,2048]{1,0:T(8,128)(2,1)} %shard_map.100) | data formatting | bytes 1048576

commit v2 on v1

--- a/solution.py
+++ b/solution.py
@@ -27,7 +27,7 @@
     out,
     normed, send, recv, result, back, v_gate, v_up, v_down, wide,
     local_sem, out_send, out_recv, ret_send, ret_recv,
-    z_send, z_recv, y_send, y_recv, x_send, x_recv, c_send, c_recv,
+    w_send, w_recv,
 ):
     n_z, n_y, n_x, n_c = dims
     plane = n_y * n_x * n_c
@@ -95,38 +95,35 @@
             device_id=(target,), device_id_type=pl.DeviceIdType.MESH,
         )
 
-    def z_copy(d, origin):
-        part = wide.at[:, origin, my_y, my_x, my_c]
-        return remote(part, part, z_send.at[d], z_recv.at[d], dev((my_z + d) % n_z, my_y, my_x, my_c))
-
-    def y_copy(d, origin):
-        part = wide.at[:, :, origin, my_x, my_c]
-        return remote(part, part, y_send.at[d], y_recv.at[d], dev(my_z, (my_y + d) % n_y, my_x, my_c))
-
-    def x_copy(d, origin):
-        part = wide.at[:, :, :, origin, my_c]
-        return remote(part, part, x_send.at[d], x_recv.at[d], dev(my_z, my_y, (my_x + d) % n_x, my_c))
-
-    def c_copy(d, origin):
-        part = wide.at[:, :, :, :, origin]
-        return remote(part, part, c_send.at[d], c_recv.at[d], dev(my_z, my_y, my_x, (my_c + d) % n_c))
-
-    stages = [(z_copy, n_z, my_z), (y_copy, n_y, my_y), (x_copy, n_x, my_x), (c_copy, n_c, my_c)]
+    at = (my_z, my_y, my_x, my_c)
+    orders = ((0, 1, 2, 3), (0, 2, 1, 3))
+
+    def block_copy(half, stage, d, incoming):
+        order = orders[half]
+        axis = order[stage]
+        origin = (at[axis] + dims[axis] - d) % dims[axis] if incoming else at[axis]
+        where = [at[i] for i in range(4)]
+        for held in order[:stage]:
+            where[held] = slice(None)
+        where[axis] = origin
+        part = wide.at[(half,) + tuple(where)]
+        target = [at[i] for i in range(4)]
+        target[axis] = (at[axis] + d) % dims[axis]
+        return remote(part, part, w_send.at[half, stage, d], w_recv.at[half, stage, d], dev(*target))
+
+    def each(stage, act, incoming=False):
+        for half in range(2):
+            for d in range(1, dims[orders[half][stage]]):
+                act(block_copy(half, stage, d, incoming))
 
     def begin(stage):
-        copy, size, at = stages[stage]
-        for d in range(1, size):
-            copy(d, at).start()
+        each(stage, lambda copy: copy.start())
 
     def arrive(stage):
-        copy, size, at = stages[stage]
-        for d in range(1, size):
-            copy(d, (at + size - d) % size).wait_recv()
+        each(stage, lambda copy: copy.wait_recv(), True)
 
     def leave(stage):
-        copy, size, at = stages[stage]
-        for d in range(1, size):
-            copy(d, at).wait_send()
+        each(stage, lambda copy: copy.wait_send())
 
     begin(0)
 
@@ -180,10 +177,14 @@
 
     for phase in range(n_z):
         do_phase(phase)
-        if phase < 3:
-            arrive(phase + 1)
-            if phase < 2:
-                begin(phase + 2)
+        if phase == 0:
+            arrive(1)
+            begin(2)
+        if phase == 2:
+            arrive(2)
+            begin(3)
+        if phase == 3:
+            arrive(3)
 
     back[me] = result[me]
 
@@ -240,8 +241,7 @@
             pltpu.VMEM((ff, width), BF16),
             pltpu.VMEM((2,) + dims + (d_rows, dh), BF16),
             dma((5,)), dma((n,)), dma((n,)), dma((n,)), dma((n,)),
-            dma((n_z,)), dma((n_z,)), dma((side,)), dma((side,)),
-            dma((side,)), dma((side,)), dma((2,)), dma((2,)),
+            dma((2, 4, n_z)), dma((2, 4, n_z)),
         ],
         compiler_params=pltpu.CompilerParams(
             collective_id=0, has_side_effects=True, vmem_limit_bytes=60 * 1024 * 1024

time: 102 us -> 79.5 us (0.78)
  Pallas kernels: 99.8 us -> 77.5 us
    pallas_call x1, Pallas kernels: 99.8 us -> 77.5 us  [on_device(): pl.pallas_call(functools.partial(kernel, dims), out_shape=jax.ShapeDtypeS...]
where the time goes in v2:
time: 79.5 us; the launch traced here: 79.4 us
  Pallas kernels  77.5 us (97%)
  local copies, waits for them, and re-layouts  1.88 us (2%)
    pallas_call x1, Pallas kernels, on_device(): pl.pallas_call(functools.partial(kernel, dims), out_shape=jax.ShapeDtypeS...  77.5 us
    unnamed x1, local copies, waits for them, and re-layouts  1.88 us

profile of v2, /device:TPU:0, one launch (start us, length us, event | category | flops | bytes accessed | tf_op | source)
XLA Modules:
  0.0 79.4 jit_solution(10254399669319603998)
XLA Ops:
  0.0 77.5 %shard_map.100 = bf16[128,2048]{1,0:T(8,128)(2,1)} custom-call(bf16[128,2048]{1,0:T(8,128)(2,1)} %tokens.1, f32[1,2048]{1,0:T(1,128)} %bitcast.6, s32[2,128]{1,0:T(2,128)} %bitcast.8, f32[2,128]{1,0:T(2,128)} %bitcast.9, bf16[1,2048,1024]{2,1,0:T(8,128)(2,1)} %w_gate.1, bf16[1,2048,1024]{2,1,0:T(8,128)(2,1)} %w_up.1, bf16[1,1024,2048]{2,1,0:T(8,128)(2,1)} %w_down.1, ...), custom_call_target="tpu_custom_call" | custom-call | tf_op jit(solution)/shard_map/pallas_call | solution.py:228
  77.5 1.9 %copy.12 = bf16[128,2048]{1,0:T(8,128)(2,1)} copy(bf16[128,2048]{1,0:T(8,128)(2,1)} %shard_map.100) | data formatting | bytes 1048576

commit v3 on v2

--- a/solution.py
+++ b/solution.py
@@ -112,9 +112,10 @@
         return remote(part, part, w_send.at[half, stage, d], w_recv.at[half, stage, d], dev(*target))
 
     def each(stage, act, incoming=False):
-        for half in range(2):
-            for d in range(1, dims[orders[half][stage]]):
-                act(block_copy(half, stage, d, incoming))
+        for d in range(1, max(dims)):
+            for half in range(2):
+                if d < dims[orders[half][stage]]:
+                    act(block_copy(half, stage, d, incoming))
 
     def begin(stage):
         each(stage, lambda copy: copy.start())
@@ -150,7 +151,10 @@
     def giveback(target, origin):
         return remote(result.at[target], back.at[origin], ret_send.at[target], ret_recv.at[origin], target)
 
-    over_others(0, n, lambda t: dispatch(t, me).start())
+    over_others(0, plane, lambda t: dispatch(t, me).start())
+    arrive(0)
+    begin(1)
+    over_others(plane, n, lambda t: dispatch(t, me).start())
     recv[me] = send[me]
 
     for load in loads:
@@ -165,9 +169,6 @@
         hidden = (gate_part / (1.0 + jnp.exp(-gate_part)) * up_part).astype(BF16)
         res = jnp.dot(hidden, v_down[...], preferred_element_type=F32)
         result[block] = res.reshape(plane, CAP, width).astype(BF16)
-
-    arrive(0)
-    begin(1)
 
     def do_phase(phase):
         lo, hi = phase * plane, (phase + 1) * plane

time: 79.5 us -> 84 us (1.057)
  the two profiles are of different devices: /device:TPU:0 before, /device:TPU:21 now
where the time goes in v3:
time: 84 us; the launch traced here: 83.9 us
  Pallas kernels  82 us (98%)
  local copies, waits for them, and re-layouts  1.88 us (2%)
    pallas_call x1, Pallas kernels, on_device(): pl.pallas_call(functools.partial(kernel, dims), out_shape=jax.ShapeDtypeS...  82 us
    unnamed x1, local copies, waits for them, and re-layouts  1.88 us

profile of v3, /device:TPU:21, one launch (start us, length us, event | category | flops | bytes accessed | tf_op | source)
XLA Modules:
  0.0 83.9 jit_solution(11134166947668617027)
XLA Ops:
  0.0 82.0 %shard_map.100 = bf16[128,2048]{1,0:T(8,128)(2,1)} custom-call(bf16[128,2048]{1,0:T(8,128)(2,1)} %tokens.1, f32[1,2048]{1,0:T(1,128)} %bitcast.6, s32[2,128]{1,0:T(2,128)} %bitcast.8, f32[2,128]{1,0:T(2,128)} %bitcast.9, bf16[1,2048,1024]{2,1,0:T(8,128)(2,1)} %w_gate.1, bf16[1,2048,1024]{2,1,0:T(8,128)(2,1)} %w_up.1, bf16[1,1024,2048]{2,1,0:T(8,128)(2,1)} %w_down.1, ...), custom_call_target="tpu_custom_call" | custom-call | tf_op jit(solution)/shard_map/pallas_call | solution.py:229
  82.0 1.9 %copy.12 = bf16[128,2048]{1,0:T(8,128)(2,1)} copy(bf16[128,2048]{1,0:T(8,128)(2,1)} %shard_map.100) | data formatting | bytes 1048576
